TPU v7x, 32 devices: a whole 2x2x4 slice. The times are simulated.
32 devices in a mesh: dp: 4 (over y, x), kv: 4 (over z), tp: 2 (over core).
Axes of the slice: x: 2, y: 2, z: 4, core: 2. Of those that a mesh axis runs over, the one named last changes fastest.
Arguments:
- tokens: bfloat16 [4, 2048, 1024], P('dp', ('kv', 'tp')), may hold values from -6 to 6
- w_query: bfloat16 [1024, 1024], P(None, 'tp'), may hold values from -0.1875 to 0.1875
- w_key: bfloat16 [1024, 256], P(None, 'tp'), may hold values from -0.1875 to 0.1875
- w_value: bfloat16 [1024, 256], P(None, 'tp'), may hold values from -0.1875 to 0.1875
- w_out: bfloat16 [1024, 1024], P('tp'), may hold values from -0.1875 to 0.1875
- chosen: int32 [4, 32, 15], P('dp', 'kv'), may hold values from -1 to 30, as said below
Outputs:
- normed: bfloat16 [4, 2048, 1024], P('dp', ('kv', 'tp'))
- logsums: float32 [4, 2048, 16], P('dp', 'kv', 'tp')
Inputs may be any that keep to these rules, and one draw needn't show every extreme that they name: Each entry of chosen[s, c] is -1 or a block below c; entries of a row that are not -1 differ. Within a sequence, the 15 times 8 entries of the query blocks of one aligned run of 8 blocks name at most 4 different blocks inside any one aligned run, and some run pair reaches exactly 4.
All inputs are finite; a program needn't handle non-finite values.
Results may differ from a plain program's by a relative error of at most 0.0085.
Values may be sent and summed in bfloat16 or wider, within the bound.
A program may use at most 64 MiB of HBM per device.

v0:
```python
import jax
import jax.numpy as jnp
from jax import lax
from jax.sharding import PartitionSpec as P

HEAD_DIM = 64
BLK = 64
PICK = 15
CAP = 4


THETA_BASE = 10000.0
NEGATIVE = -1e30
EPSILON = 1e-06


def gathered_then(x, axis, dim, block):
    whole = lax.all_gather(x, axis, axis=dim, tiled=True)
    return block(whole, jnp.int32(0))


def own_rows(term, width, axis):
    whole = term(jnp.int32(0), width * lax.axis_size(axis))
    return lax.psum_scatter(whole, axis, scatter_dimension=0, tiled=True)


def rotate(values_in, positions):
    half_width = values_in.shape[-1] // 2
    inverse = THETA_BASE ** (-jnp.arange(half_width, dtype=jnp.float32) / half_width)
    angles = positions.astype(jnp.float32)[:, None] * inverse[None, :]
    cosine_table = jnp.cos(angles)[:, None, :]
    sine_table = jnp.sin(angles)[:, None, :]
    as_float = values_in.astype(jnp.float32)
    first_half = as_float[..., :half_width]
    second_half = as_float[..., half_width:]
    joined = jnp.concatenate(
        [
            first_half * cosine_table - second_half * sine_table,
            second_half * cosine_table + first_half * sine_table,
        ],
        axis=-1,
    )
    return joined.astype(jnp.bfloat16)


def want_table(chosen_rows, owner_count, local_blocks):
    usable = chosen_rows >= 0
    flat_picks = jnp.where(usable, chosen_rows, 0).reshape(-1)
    counts = jax.ops.segment_sum(
        usable.astype(jnp.int32).reshape(-1), flat_picks, num_segments=owner_count * local_blocks
    )
    needed = (counts > 0).astype(jnp.int32).reshape(owner_count, local_blocks)
    ranking = jnp.cumsum(needed, axis=1) - 1
    matches = (needed[:, :, None] == 1) & (
        ranking[:, :, None] == jnp.arange(CAP, dtype=jnp.int32)[None, None, :]
    )
    local_index = jnp.arange(local_blocks, dtype=jnp.int32)[None, :, None]
    wanted = jnp.sum(jnp.where(matches, local_index, 0), axis=1)
    present = jnp.any(matches, axis=1)
    return (jnp.where(present, wanted, -1).astype(jnp.int32), ranking.astype(jnp.int32))


def block_mask(usable_picks):
    picked_keys = jnp.repeat(usable_picks, BLK)
    earlier = jnp.broadcast_to(picked_keys[None, :], (BLK, PICK * BLK))
    query_pos = jnp.arange(BLK, dtype=jnp.int32)
    causal = query_pos[None, :] <= query_pos[:, None]
    return jnp.concatenate([earlier, causal], axis=1)


def shards(tokens, w_query, w_key, w_value, w_out, chosen):
    query_width = w_query.shape[1]
    key_width = w_key.shape[1]
    head_count = query_width // HEAD_DIM
    kv_count = key_width // HEAD_DIM
    group_size = head_count // kv_count

    def project(token_piece, first_row):
        return jnp.concatenate(
            [
                jnp.dot(token_piece, w_query, preferred_element_type=jnp.float32).astype(
                    jnp.bfloat16
                ),
                jnp.dot(token_piece, w_key, preferred_element_type=jnp.float32).astype(
                    jnp.bfloat16
                ),
                jnp.dot(token_piece, w_value, preferred_element_type=jnp.float32).astype(
                    jnp.bfloat16
                ),
            ],
            axis=1,
        )

    projections = gathered_then(tokens[0], "tp", 0, project)
    token_count = projections.shape[0]
    my_index = lax.axis_index("kv")
    owner_count = lax.axis_size("kv")
    local_blocks = token_count // BLK
    positions = my_index * token_count + jnp.arange(token_count, dtype=jnp.int32)
    queries = rotate(
        projections[:, :query_width].reshape(token_count, head_count, HEAD_DIM), positions
    )
    key_rows = rotate(
        projections[:, query_width : query_width + key_width].reshape(
            token_count, kv_count, HEAD_DIM
        ),
        positions,
    )
    value_rows = projections[:, query_width + key_width :].reshape(token_count, kv_count, HEAD_DIM)
    query_blocks = queries.reshape(local_blocks, BLK, kv_count, group_size, HEAD_DIM)
    key_blocks = key_rows.reshape(local_blocks, BLK, kv_count, HEAD_DIM)
    value_blocks = value_rows.reshape(local_blocks, BLK, kv_count, HEAD_DIM)
    chosen_rows = chosen[0]
    wanted, ranking = want_table(chosen_rows, owner_count, local_blocks)
    asked = lax.all_to_all(wanted + 1, "kv", split_axis=0, concat_axis=0, tiled=True) - 1
    safe_asked = jnp.maximum(asked, 0)
    present = (asked >= 0)[:, :, None, None, None]
    send_keys = jnp.where(present, key_blocks[safe_asked], jnp.zeros((), jnp.bfloat16))
    send_values = jnp.where(present, value_blocks[safe_asked], jnp.zeros((), jnp.bfloat16))
    got_keys = lax.all_to_all(send_keys, "kv", split_axis=0, concat_axis=0, tiled=True)
    got_values = lax.all_to_all(send_values, "kv", split_axis=0, concat_axis=0, tiled=True)
    got_keys = got_keys.reshape(owner_count * CAP, BLK, kv_count, HEAD_DIM)
    got_values = got_values.reshape(owner_count * CAP, BLK, kv_count, HEAD_DIM)
    usable_all = chosen_rows >= 0
    safe_picks = jnp.where(usable_all, chosen_rows, 0)
    slot_index = safe_picks // local_blocks * CAP + ranking.reshape(-1)[safe_picks]

    def one_block(item):
        block_queries, own_keys, own_values, block_slots, usable_picks = item
        gathered_keys = jnp.concatenate(
            [got_keys[block_slots].reshape(PICK * BLK, kv_count, HEAD_DIM), own_keys], axis=0
        )
        gathered_values = jnp.concatenate(
            [got_values[block_slots].reshape(PICK * BLK, kv_count, HEAD_DIM), own_values], axis=0
        )
        scores = jnp.einsum(
            "qkgd,nkd->kgqn", block_queries, gathered_keys, preferred_element_type=jnp.float32
        )
        scores = scores * HEAD_DIM ** (-0.5)
        scores = jnp.where(block_mask(usable_picks)[None, None], scores, NEGATIVE)
        maximum = jnp.max(scores, axis=-1, keepdims=True)
        exponent = jnp.exp(scores - maximum)
        denominator = jnp.sum(exponent, axis=-1, keepdims=True)
        logsum = (maximum + jnp.log(denominator))[..., 0]
        weights = (exponent / denominator).astype(jnp.bfloat16)
        combined = jnp.einsum(
            "kgqn,nkd->qkgd", weights, gathered_values, preferred_element_type=jnp.float32
        )
        return (
            combined.astype(jnp.bfloat16).reshape(BLK, -1),
            jnp.transpose(logsum, (2, 0, 1)).reshape(BLK, -1),
        )

    outputs, block_logs = lax.map(
        one_block, (query_blocks, key_blocks, value_blocks, slot_index, usable_all)
    )
    attended = outputs.reshape(token_count, head_count * HEAD_DIM)

    def head_term(first_row, row_count):
        rows_part = lax.dynamic_slice_in_dim(attended, first_row, row_count, 0)
        return jnp.dot(rows_part, w_out, preferred_element_type=jnp.float32)

    projected = own_rows(head_term, token_count // lax.axis_size("tp"), "tp")
    scale_rows = lax.rsqrt(jnp.mean(projected * projected, axis=-1, keepdims=True) + EPSILON)
    normed = (projected * scale_rows).astype(jnp.bfloat16)
    return (normed[None], block_logs.reshape(token_count, head_count)[None])


def solution(mesh):
    placed = (
        P("dp", ("kv", "tp"), None),
        P(None, "tp"),
        P(None, "tp"),
        P(None, "tp"),
        P("tp", None),
        P("dp", "kv", None),
    )
    return jax.shard_map(
        shards,
        mesh=mesh,
        in_specs=placed,
        out_specs=(P("dp", ("kv", "tp"), None), P("dp", "kv", "tp")),
        check_vma=False,
    )
```

profile of v0, /device:TPU:27, one launch (start us, length us, event | category | flops | bytes accessed | tf_op | source)
XLA Modules:
  0.0 159.1 jit_solution(1542739241134124419)
XLA Ops:
  12.0 4.5 %all-to-all-start = ((s32[4,1,4]{2,1,0:T(1,128)}), s32[4,1,4]{2,1,0:T(1,128)S(1)}, u32[]{:S(2)}, u32[]{:S(2)}) async-start(s32[4,1,4]{2,1,0:T(1,128)} %bitcast.21), calls=%async_computation | async-start | bytes 4096 | tf_op jit(solution)/shard_map/all_to_all | solution.py:115
  20.3 1.8 %convolution_convert_fusion.2 = bf16[512,128]{0,1:T(8,128)(2,1)S(1)} fusion(bf16[1024,128]{1,0:T(8,128)(2,1)S(1)} %copy-done.4, bf16[1,512,1024]{2,1,0:T(8,128)(2,1)} %all-gather.3.cloned.1.call-done), kind=kOutput, calls=%fused_computation.35 | convolution fusion | flops 134283264 | bytes 1441792 | tf_op jit(solution)/shard_map/dot_general | solution.py:84
  24.3 2.6 %gather_fusion.3 = bf16[16,64,2,64]{3,2,1,0:T(2,128)(2,1)S(1)} fusion(bf16[8,64,2,64]{3,2,1,0:T(2,128)(2,1)} %reshape_reshape.3, s32[1024]{0:T(1024)S(1)} %pad_clamp_fusion.1), kind=kCustom, calls=%fused_computation.3 | custom fusion | bytes 524352 | tf_op jit(solution)/shard_map/gather | solution.py:119
  28.3 2.0 %broadcast_select_fusion = (bf16[4,4,64,2,64]{4,2,3,1,0:T(8,128)(2,1)}, bf16[4,4,64,2,64]{4,2,3,1,0:T(8,128)(2,1)S(1)}) fusion(bf16[4,4,64,2,64]{4,2,3,1,0:T(8,128)(2,1)} %bitcast.137, pred[4,4]{1,0:T(4,128)(4,1)S(1)} %bitcast.149, bf16[4,4,64,2,64]{4,3,2,1,0:T(2,128)(2,1)S(1)} %bitcast.136), kind=kLoop, calls=%fused_computation.47 | loop fusion | flops 262144 | bytes 1048592 | tf_op jit(solution)/shard_map/jit(_where)/select_n | solution.py:118
  30.3 2.1 %reshape.341 = bf16[4,2,16384]{2,1,0:T(2,128)(2,1)} reshape(bf16[4,4,2,64,64]{4,3,2,1,0:T(8,128)(2,1)} %bitcast.138) | data formatting | bytes 524288
  32.4 4.5 %all-to-all-start.2 = ((bf16[4,2,16384]{2,1,0:T(2,128)(2,1)}), bf16[4,2,16384]{2,1,0:T(2,128)(2,1)S(1)}, u32[]{:S(2)}, u32[]{:S(2)}) async-start(bf16[4,2,16384]{2,1,0:T(2,128)(2,1)} %reshape.341), calls=%async_computation.2 | async-start | bytes 524288 | tf_op jit(solution)/shard_map/all_to_all | solution.py:120
  38.1 4.9 %all-to-all-done.2 = bf16[4,2,16384]{2,1,0:T(2,128)(2,1)S(1)} async-done(((bf16[4,2,16384]{2,1,0:T(2,128)(2,1)}), bf16[4,2,16384]{2,1,0:T(2,128)(2,1)S(1)}, u32[]{:S(2)}, u32[]{:S(2)}) %all-to-all-start.2) | async-done | bytes 262176 | tf_op jit(solution)/shard_map/all_to_all | solution.py:120
  43.0 7.2 %all-to-all-start.1 = ((bf16[4,2,16384]{2,1,0:T(2,128)(2,1)}), bf16[4,2,16384]{2,1,0:T(2,128)(2,1)}, u32[]{:S(2)}, u32[]{:S(2)}) async-start(bf16[4,2,16384]{2,1,0:T(2,128)(2,1)} %reshape.339), calls=%async_computation.1 | async-start | bytes 524288 | tf_op jit(solution)/shard_map/all_to_all | solution.py:121
  50.2 2.0 %convolution_convert_fusion.1 = bf16[512,512]{0,1:T(8,128)(2,1)S(1)} fusion(bf16[1024,512]{1,0:T(8,128)(2,1)} %param.9, bf16[1,512,1024]{2,1,0:T(8,128)(2,1)S(1)} %copy-done.1), kind=kOutput, calls=%fused_computation.34 | convolution fusion | flops 537133056 | bytes 2621440 | tf_op jit(solution)/shard_map/dot_general | solution.py:81
  53.3 1.6 %copy.73 = bf16[8,64,2,4,64]{4,1,3,2,0:T(8,128)(2,1)} copy(bf16[8,64,2,4,64]{1,0,4,3,2:T(8,128)(2,1)S(1)} %pad_maximum_fusion) | data formatting | bytes 1048576 | tf_op jit(solution)/shard_map/while | solution.py:154
  58.4 74.9 %while.12 = (s32[]{:T(128)}, bf16[8,64,512]{2,1,0:T(8,128)(2,1)}, f32[8,64,8]{1,0,2:T(8,128)S(1)}, s32[8,15]{1,0:T(8,128)S(1)}, bf16[16,64,2,64]{3,2,1,0:T(2,128...) while((s32[]{:T(128)}, bf16[8,64,512]{2,1,0:T(8,128)(2,1)}, ...), condition=%wide.region_7.8_spmd, body=%wide.region_4.7_spmd.sunk | while | flops 139563568 | bytes 9541883 | solution.py:154
  59.7 1.5 gather_fusion.1
  62.0 1.5 gather_fusion
  69.1 1.5 gather_fusion.1
  71.4 1.5 gather_fusion
  78.5 1.5 gather_fusion.1
  80.7 1.5 gather_fusion
  87.8 1.5 gather_fusion.1
  90.1 1.5 gather_fusion
  92.3 1.4 fusion.36
  97.2 1.5 gather_fusion.1
  99.4 1.5 gather_fusion
  106.5 1.5 gather_fusion.1
  108.8 1.5 gather_fusion
  115.9 1.5 gather_fusion.1
  118.2 1.5 gather_fusion
  120.4 1.4 fusion.36
  125.3 1.5 gather_fusion.1
  127.5 1.5 gather_fusion
  133.3 3.1 %fusion.26 = f32[512,1024]{1,0:T(8,128)} fusion(bf16[512,512]{1,0:T(8,128)(2,1)} %bitcast.143, bf16[512,1024]{1,0:T(8,128)(2,1)S(1)} %copy-done), kind=kOutput, calls=%fused_computation.88 | convolution fusion | flops 536870912 | bytes 3670016 | tf_op jit(solution)/shard_map/dot_general | solution.py:161
  137.1 11.6 %reduce-scatter.2.cloned.1.call-done = f32[256,1024]{1,0:T(8,128)} async-done(((f32[512,1024]{1,0:T(8,128)}), f32[256,1024]{1,0:T(8,128)}) %reduce-scatter.2.cloned.1.call-update) | async-done | bytes 1048592 | tf_op jit(solution)/shard_map/reduce_scatter | solution.py:24
  150.1 2.1 %fusion.15 = bf16[1,256,1024]{2,1,0:T(8,128)(2,1)} fusion(f32[256,1024]{1,0:T(8,128)} %reduce-scatter.2.cloned.1.call-done, f32[256]{0:T(256)S(1)} %add_rsqrt_fusion), kind=kLoop, calls=%fused_computation.43 | loop fusion | flops 524288 | bytes 1573888 | tf_op jit(solution)/shard_map/broadcast_in_dim | solution.py:166
  (243 shorter events, 66.5 us)
Async XLA Ops:
  7.2 126.2 %copy-start = (bf16[512,1024]{1,0:T(8,128)(2,1)S(1)}, bf16[512,1024]{1,0:T(8,128)(2,1)}, u32[]{:S(2)}) copy-start(bf16[512,1024]{1,0:T(8,128)(2,1)} %param.12) | copy-start | bytes 3145732
  7.2 13.1 %all-gather.3.cloned.1.call-start = ((), (), s32[]{:S(2)}) async-start(), calls=%async_computation.5 | async-start | bytes 1572864 | tf_op jit(solution)/shard_map/all_gather | solution.py:18
  12.0 7.1 %all-to-all-start = ((s32[4,1,4]{2,1,0:T(1,128)}), s32[4,1,4]{2,1,0:T(1,128)S(1)}, u32[]{:S(2)}, u32[]{:S(2)}) async-start(s32[4,1,4]{2,1,0:T(1,128)} %bitcast.21), calls=%async_computation | async-start | bytes 4096 | tf_op jit(solution)/shard_map/all_to_all | solution.py:115
  17.4 2.9 %copy-start.4 = (bf16[1024,128]{1,0:T(8,128)(2,1)S(1)}, bf16[1024,128]{1,0:T(8,128)(2,1)}, u32[]{:S(2)}) copy-start(bf16[1024,128]{1,0:T(8,128)(2,1)} %param.10) | copy-start | bytes 786436
  18.7 4.2 %copy-start.5 = (bf16[1024,128]{1,0:T(8,128)(2,1)S(1)}, bf16[1024,128]{1,0:T(8,128)(2,1)}, u32[]{:S(2)}) copy-start(bf16[1024,128]{1,0:T(8,128)(2,1)} %param.11) | copy-start | bytes 786436
  20.3 2.6 %copy-start.1 = (bf16[1,512,1024]{2,1,0:T(8,128)(2,1)S(1)}, bf16[1,512,1024]{2,1,0:T(8,128)(2,1)}, u32[]{:S(2)}) copy-start(bf16[1,512,1024]{2,1,0:T(8,128)(2,1)} %all-gather.3.cloned.1.call-done) | copy-start | bytes 3145732
  26.9 10.1 %copy-start.6 = (s32[1,8,15]{2,1,0:T(8,128)S(1)}, s32[1,8,15]{2,1,0:T(8,128)}, u32[]{:S(2)}) copy-start(s32[1,8,15]{2,1,0:T(8,128)} %param.13) | copy-start | bytes 1444
  32.4 10.6 %all-to-all-start.2 = ((bf16[4,2,16384]{2,1,0:T(2,128)(2,1)}), bf16[4,2,16384]{2,1,0:T(2,128)(2,1)S(1)}, u32[]{:S(2)}, u32[]{:S(2)}) async-start(bf16[4,2,16384]{2,1,0:T(2,128)(2,1)} %reshape.341), calls=%async_computation.2 | async-start | bytes 524288 | tf_op jit(solution)/shard_map/all_to_all | solution.py:120
  43.0 9.3 %copy-start.2 = (bf16[4,2,16384]{2,1,0:T(2,128)(2,1)}, bf16[4,2,16384]{2,1,0:T(2,128)(2,1)S(1)}, u32[]{:S(2)}) copy-start(bf16[4,2,16384]{2,1,0:T(2,128)(2,1)S(1)} %all-to-all-done.2) | copy-start | bytes 786436
  43.0 13.5 %all-to-all-start.1 = ((bf16[4,2,16384]{2,1,0:T(2,128)(2,1)}), bf16[4,2,16384]{2,1,0:T(2,128)(2,1)}, u32[]{:S(2)}, u32[]{:S(2)}) async-start(bf16[4,2,16384]{2,1,0:T(2,128)(2,1)} %reshape.339), calls=%async_computation.1 | async-start | bytes 524288 | tf_op jit(solution)/shard_map/all_to_all | solution.py:121
  50.2 98.5 %reduce-scatter.2.cloned.1.call-start = ((), (), s32[]{:S(2)}) async-start(), calls=%async_computation.4 | async-start | bytes 3145728 | tf_op jit(solution)/shard_map/reduce_scatter | solution.py:24
  53.3 1.6 %copy-start.3 = (bf16[4,2,16384]{2,1,0:T(2,128)(2,1)S(1)}, bf16[4,2,16384]{2,1,0:T(2,128)(2,1)}, u32[]{:S(2)}) copy-start(bf16[4,2,16384]{2,1,0:T(2,128)(2,1)} %copy-done.2) | copy-start | bytes 786436
  54.9 3.5 %copy-start.7 = (f32[8,64,8]{1,0,2:T(8,128)S(1)}, f32[8,64,8]{1,0,2:T(8,128)}, u32[]{:S(2)}) copy-start(f32[8,64,8]{1,0,2:T(8,128)} %custom-call.11) | copy-start | bytes 49156
Sparse Core Ops, SparseCore 0:
  9.5 10.6 all-gather.2
  136.6 12.1 reduce-scatter.1
where the time goes:
time: 162 us; the launch traced here: 159 us
  local copies, waits for them, and re-layouts  68.4 us (42%)
  matrix products  24.8 us (15%)
  waiting for transfers between devices  19 us (12%)
  starting transfers between devices  16.3 us (10%)
  other arithmetic  15.5 us (10%)
  between operations  14.3 us (9%)
    gather x8, local copies, waits for them, and re-layouts, one_block(): got_values[block_slots].reshape(PICK * BLK, kv_count, HEAD_DIM)  12.3 us
    gather x8, local copies, waits for them, and re-layouts, one_block(): got_keys[block_slots].reshape(PICK * BLK, kv_count, HEAD_DIM)  12.3 us
    reduce_scatter x1, waiting for transfers between devices, own_rows(): return lax.psum_scatter(whole, axis, scatter_dimension=0, tiled=True)  11.6 us
    dot_general x8, matrix products, one_block(): jnp.einsum('qkgd,nkd->kgqn', block_queries, gathered_keys, preferred_elem...  11.5 us
    dynamic_slice x32, local copies, waits for them, and re-layouts, shards(): lax.map(one_block, (query_blocks, key_blocks, value_blocks, slot_index, u...  7.96 us
    all_to_all x1, starting transfers between devices, shards(): lax.all_to_all(send_values, 'kv', split_axis=0, concat_axis=0, tiled=True)  7.17 us
    dynamic_update_slice x24, local copies, waits for them, and re-layouts, shards(): lax.map(one_block, (query_blocks, key_blocks, value_blocks, slot_index, u...  6.21 us
    dot_general x8, matrix products, one_block(): jnp.einsum('kgqn,nkd->qkgd', weights, gathered_values, preferred_element_...  5.99 us
  transfers between devices with their start and end apart: 5, of which 4 were waited for; matrix products, arithmetic and copies ran while one was open for 9% of the time, Pallas kernels for 0%

commit v1 on v0

v1 whole, which is shorter than its diff:
```python
import functools
import math

import jax
import jax.numpy as jnp
from jax import lax
from jax.experimental import pallas as pl
from jax.experimental.pallas import tpu as pltpu
from jax.sharding import PartitionSpec as P

HEAD_DIM = 64
BLK = 64
CAP = 4
THETA_BASE = 10000.0
NEGATIVE = -1e30
EPSILON = 1e-06
MESH = pl.DeviceIdType.MESH
F32 = jnp.float32
BF16 = jnp.bfloat16
NT = (((1,), (1,)), ((), ()))
NN = (((1,), (0,)), ((), ()))


def mm(a, b, dims=NN):
    return lax.dot_general(a, b, dims, preferred_element_type=F32)


def iota(shape, dim):
    return lax.broadcasted_iota(jnp.int32, shape, dim)


def kernel(
    n,
    chosen_ref,
    tokens_hbm,
    wq_hbm,
    wk_hbm,
    wv_hbm,
    wo_hbm,
    normed_ref,
    logs_ref,
    tok,
    wq,
    wkv,
    wo,
    cos_t,
    sin_t,
    pick,
    bias,
    keys,
    vals_t,
    sel_k,
    sel_v,
    got_k,
    got_v,
    qaug,
    m_s,
    l_s,
    acc,
    att,
    send_p,
    recv_p,
    load_sem,
    tok_sem,
    pick_send,
    pick_recv,
    k_send,
    k_recv,
    v_send,
    v_recv,
    p_send,
    p_recv,
):
    me = lax.axis_index("kv")
    half = lax.axis_index("tp")
    other = 1 - half
    rows = tok.shape[0]
    mine = rows // 2
    blocks = rows // BLK
    groups = wq.shape[1] // (2 * HEAD_DIM)
    slot_keys = CAP * BLK
    lanes_all = groups * BLK

    own_rows = pl.ds(pl.multiple_of(half * mine, mine), mine)
    ld_tok = pltpu.make_async_copy(tokens_hbm.at[0], tok.at[own_rows], load_sem.at[0])
    ld_k = pltpu.make_async_copy(wk_hbm, wkv.at[:, 0:128], load_sem.at[1])
    ld_v = pltpu.make_async_copy(wv_hbm, wkv.at[:, 128:256], load_sem.at[2])
    ld_q = pltpu.make_async_copy(wq_hbm, wq, load_sem.at[3])
    ld_tok.start()
    ld_k.start()
    ld_v.start()
    ld_q.start()
    ld_o = []
    for h in range(2):
        for g in range(groups):
            source = (h * groups + g) * HEAD_DIM
            target = (g * 2 + h) * HEAD_DIM
            ld_o.append(
                pltpu.make_async_copy(
                    wo_hbm.at[source : source + HEAD_DIM],
                    wo.at[target : target + HEAD_DIM],
                    load_sem.at[4 + h * groups + g],
                )
            )
    for copy in ld_o:
        copy.start()

    barrier = pltpu.get_barrier_semaphore()
    pl.semaphore_signal(barrier, inc=1, device_id={"tp": other}, device_id_type=MESH)
    for d in range(1, n):
        pl.semaphore_signal(
            barrier, inc=1, device_id={"kv": lax.rem(me + d, n)}, device_id_type=MESH
        )

    npad = pick.shape[2]
    chosen = chosen_ref[0]
    block_ids = iota((blocks, npad), 1)
    picked = jnp.zeros((blocks, npad), F32)
    for k in range(chosen.shape[1]):
        picked = picked + (chosen[:, k : k + 1] == block_ids).astype(F32)
    pick[0] = picked

    pl.semaphore_wait(barrier, n)
    ld_tok.wait()
    tok_copy = pltpu.make_async_remote_copy(
        src_ref=tok.at[own_rows],
        dst_ref=tok.at[own_rows],
        send_sem=tok_sem.at[0],
        recv_sem=tok_sem.at[1],
        device_id={"tp": other},
        device_id_type=MESH,
    )
    tok_copy.start()

    def pick_copy(d, target):
        return pltpu.make_async_remote_copy(
            src_ref=pick.at[0],
            dst_ref=pick.at[d],
            send_sem=pick_send.at[d],
            recv_sem=pick_recv.at[d],
            device_id={"kv": target},
            device_id_type=MESH,
        )

    @pl.loop(1, me + 1)
    def _(d):
        pick_copy(d, me - d).start()

    lane = iota((1, 128), 1)
    inverse = jnp.exp((lane % 32).astype(F32) * (-math.log(THETA_BASE) / 32))
    sign = jnp.where(lane % 64 < 32, -1.0, 1.0)
    inner = iota((BLK, 128), 0).astype(F32) * inverse
    cos_in, sin_in = jnp.cos(inner), jnp.sin(inner)
    starts = (me * rows + iota((blocks, 128), 0) * BLK).astype(F32) * inverse
    cos_st, sin_st = jnp.cos(starts), jnp.sin(starts)
    for c in range(blocks):
        part = slice(c * BLK, (c + 1) * BLK)
        cs, sn = cos_st[c : c + 1], sin_st[c : c + 1]
        cos_t[part] = cs * cos_in - sn * sin_in
        sin_t[part] = (sn * cos_in + cs * sin_in) * sign

    slots = bias.shape[0]
    nslots = slots // slot_keys * CAP

    def slot_table(marks):
        needed = (jnp.max(marks, axis=0, keepdims=True) > 0).astype(F32)
        b_in, b_out = iota((npad, npad), 0), iota((npad, npad), 1)
        before = ((b_in // blocks == b_out // blocks) & (b_in < b_out)).astype(BF16)
        rank = mm(jnp.broadcast_to(needed, (8, npad)).astype(BF16), before)[0:1]
        rank = rank.astype(jnp.int32)
        place = iota((1, npad), 1) // blocks * CAP + rank
        fits = (needed > 0) & (rank < CAP)
        return jnp.where((iota((nslots, npad), 0) == place) & fits, 1.0, 0.0).astype(BF16)

    table = slot_table(picked)
    zero_rows = jnp.zeros((HEAD_DIM - blocks, npad), F32)
    twice = jnp.concatenate([picked, zero_rows, picked, zero_rows], axis=0).astype(BF16)
    reads = mm(table, twice, NT)
    lane_n = iota((nslots, 128), 1)
    reads = jnp.where(lane_n % 64 < blocks, (1.0 - reads) * NEGATIVE, 0.0).astype(BF16)
    spread = (iota((slots, nslots), 0) // BLK == iota((slots, nslots), 1)).astype(BF16)
    bias[...] = mm(spread, reads).astype(BF16)

    def rope(x, part):
        turned = jnp.where(
            iota(x.shape, 1) % 64 < 32, pltpu.roll(x, 96, 1), pltpu.roll(x, 32, 1)
        )
        return x * cos_t[part] + turned * sin_t[part]

    ld_k.wait()
    ld_v.wait()

    def project_kv(part):
        out = mm(tok[part], wkv[...]).astype(BF16)
        keys[part] = rope(out[:, 0:128].astype(F32), part).astype(BF16)
        return out[:, 128:256]

    mine_part = pl.ds(pl.multiple_of(half * mine, mine), mine)
    other_part = pl.ds(pl.multiple_of(other * mine, mine), mine)
    v_mine = project_kv(mine_part).astype(F32).T.astype(BF16)
    vals_t[:, mine_part] = v_mine
    tok_copy.wait_recv()
    v_other = project_kv(other_part).astype(F32).T.astype(BF16)
    vals_t[:, other_part] = v_other

    def select(tab, d):
        first = (
            iota((slot_keys, nslots), 1) == me * CAP + iota((slot_keys, nslots), 0) // BLK
        ).astype(BF16)
        last = (iota((npad, rows), 0) == me * blocks + iota((npad, rows), 1) // BLK).astype(BF16)
        chain = mm(mm(first, tab).astype(BF16), last)
        same = iota((slot_keys, rows), 0) % BLK == iota((slot_keys, rows), 1) % BLK
        hot = jnp.where(same, chain, 0.0).astype(BF16)
        sel_k[d] = mm(hot, keys[...]).astype(BF16)
        sel_v[d] = mm(vals_t[...], hot, NT).astype(BF16)

    def key_copy(d, target):
        return pltpu.make_async_remote_copy(
            src_ref=sel_k.at[d],
            dst_ref=got_k.at[d],
            send_sem=k_send.at[d],
            recv_sem=k_recv.at[d],
            device_id={"kv": target},
            device_id_type=MESH,
        )

    def value_copy(d, target):
        return pltpu.make_async_remote_copy(
            src_ref=sel_v.at[d],
            dst_ref=got_v.at[d],
            send_sem=v_send.at[d],
            recv_sem=v_recv.at[d],
            device_id={"kv": target},
            device_id_type=MESH,
        )

    @pl.loop(1, n - me)
    def _(d):
        pick_copy(d, me).wait_recv()
        select(slot_table(pick[d]), d)
        key_copy(d, me + d).start()
        value_copy(d, me + d).start()

    select(table, 0)

    ld_q.wait()

    @pl.loop(0, blocks)
    def _(c):
        part = pl.ds(pl.multiple_of(c * BLK, BLK), BLK)
        q = mm(tok[part], wq[...]).astype(BF16).astype(F32)
        tiles = [
            rope(q[:, t * 128 : (t + 1) * 128], part) * HEAD_DIM**-0.5 for t in range(groups)
        ]
        low = iota((BLK, 128), 1) < 64
        hot = (iota((BLK, 128), 1) % 64 == c).astype(F32)
        for g in range(groups):
            a, b = tiles[g // 2], tiles[groups // 2 + g // 2]
            if g % 2 == 0:
                both = jnp.where(low, a, pltpu.roll(b, 64, 1))
            else:
                both = jnp.where(low, pltpu.roll(a, 64, 1), b)
            place = slice(g * BLK, (g + 1) * BLK)
            qaug[c, 0, place] = jnp.where(low, both, hot).astype(BF16)
            qaug[c, 1, place] = jnp.where(low, hot, both).astype(BF16)

    def widened(k, extra, h):
        low = iota(k.shape, 1) < 64
        return jnp.where(low, k, extra) if h == 0 else jnp.where(low, extra, k)

    own_bias = bias[pl.ds(pl.multiple_of(me * slot_keys, slot_keys), slot_keys)]

    @pl.loop(0, blocks)
    def _(c):
        part = pl.ds(pl.multiple_of(c * BLK, BLK), BLK)
        for h in range(2):
            q = qaug[c, h]
            s = mm(widened(sel_k[0], own_bias, h), q, NT)
            k_own = keys[part]
            s_own = mm(widened(k_own, jnp.zeros_like(k_own), h), q, NT)
            ok = iota((BLK, lanes_all), 0) <= iota((BLK, lanes_all), 1) % BLK
            s_own = jnp.where(ok, s_own, NEGATIVE)
            m = jnp.maximum(
                jnp.max(s, axis=0, keepdims=True), jnp.max(s_own, axis=0, keepdims=True)
            )
            p = jnp.exp(s - m)
            p_own = jnp.exp(s_own - m)
            m_s[c, h] = m
            l_s[c, h] = jnp.sum(p, axis=0, keepdims=True) + jnp.sum(p_own, axis=0, keepdims=True)
            head = slice(h * HEAD_DIM, (h + 1) * HEAD_DIM)
            block_hot = (
                iota((BLK, rows), 1) == c * BLK + iota((BLK, rows), 0)
            ).astype(BF16)
            v_own = mm(vals_t[head], block_hot, NT).astype(BF16)
            acc[c, h] = mm(sel_v[0, head], p.astype(BF16)) + mm(v_own, p_own.astype(BF16))

    @pl.loop(1, me + 1)
    def _(d):
        key_copy(d, me).wait_recv()
        value_copy(d, me).wait_recv()
        owner = me - d
        extra = bias[pl.ds(pl.multiple_of(owner * slot_keys, slot_keys), slot_keys)]
        ks = [widened(got_k[d], extra, h) for h in range(2)]

        @pl.loop(0, blocks)
        def _(c):
            for h in range(2):
                s = mm(ks[h], qaug[c, h], NT)
                m_old = m_s[c, h]
                m = jnp.maximum(m_old, jnp.max(s, axis=0, keepdims=True))
                shrink = jnp.exp(m_old - m)
                p = jnp.exp(s - m)
                m_s[c, h] = m
                l_s[c, h] = l_s[c, h] * shrink + jnp.sum(p, axis=0, keepdims=True)
                head = slice(h * HEAD_DIM, (h + 1) * HEAD_DIM)
                acc[c, h] = acc[c, h] * shrink + mm(got_v[d, head], p.astype(BF16))

    @pl.loop(0, blocks)
    def _(c):
        part = pl.ds(pl.multiple_of(c * BLK, BLK), BLK)
        sums = [l_s[c, h] for h in range(2)]
        both = jnp.concatenate([acc[c, h] / sums[h] for h in range(2)], axis=0).T
        for g in range(groups):
            att[part, g * 128 : (g + 1) * 128] = both[g * BLK : (g + 1) * BLK].astype(BF16)
        logs = [m_s[c, h] + jnp.log(sums[h]) for h in range(2)]
        stacked = jnp.concatenate(
            [logs[h][:, g * BLK : (g + 1) * BLK] for h in range(2) for g in range(groups)],
            axis=0,
        )
        logs_ref[0, part] = stacked.T

    for copy in ld_o:
        copy.wait()
    pieces = send_p.shape[0]
    step = mine // pieces

    def sum_copy(i):
        return pltpu.make_async_remote_copy(
            src_ref=send_p.at[i],
            dst_ref=recv_p.at[i],
            send_sem=p_send.at[i],
            recv_sem=p_recv.at[i],
            device_id={"tp": other},
            device_id_type=MESH,
        )

    for i in range(pieces):
        part = pl.ds(pl.multiple_of(other * mine + i * step, step), step)
        send_p[i] = mm(att[part], wo[...])
        sum_copy(i).start()
    for i in range(pieces):
        part = pl.ds(pl.multiple_of(half * mine + i * step, step), step)
        own = mm(att[part], wo[...])
        sum_copy(i).wait_recv()
        total = own + recv_p[i]
        scale = lax.rsqrt(jnp.mean(total * total, axis=-1, keepdims=True) + EPSILON)
        normed_ref[0, i * step : (i + 1) * step] = (total * scale).astype(BF16)

    tok_copy.wait_send()
    for i in range(pieces):
        sum_copy(i).wait_send()

    @pl.loop(1, me + 1)
    def _(d):
        pick_copy(d, me).wait_send()

    @pl.loop(1, n - me)
    def _(d):
        key_copy(d, me).wait_send()
        value_copy(d, me).wait_send()


def shards(tokens, w_query, w_key, w_value, w_out, chosen):
    n = lax.axis_size("kv")
    mine, width = tokens.shape[1], tokens.shape[2]
    rows = 2 * mine
    blocks = rows // BLK
    heads = w_query.shape[1] // HEAD_DIM
    groups = heads // 2
    npad = -(-n * blocks // 128) * 128
    slot_keys = CAP * BLK
    lanes_all = groups * BLK
    pieces = 2
    dma = pltpu.SemaphoreType.DMA
    vmem = pl.BlockSpec(memory_space=pltpu.VMEM)
    hbm = pl.BlockSpec(memory_space=pl.ANY)
    return pl.pallas_call(
        functools.partial(kernel, n),
        out_shape=(
            jax.ShapeDtypeStruct((1, mine, width), BF16),
            jax.ShapeDtypeStruct((1, rows, heads), F32),
        ),
        in_specs=[vmem, hbm, hbm, hbm, hbm, hbm],
        out_specs=(vmem, vmem),
        scratch_shapes=[
            pltpu.VMEM((rows, width), BF16),
            pltpu.VMEM(w_query.shape, BF16),
            pltpu.VMEM((width, 256), BF16),
            pltpu.VMEM(w_out.shape, BF16),
            pltpu.VMEM((rows, 128), F32),
            pltpu.VMEM((rows, 128), F32),
            pltpu.VMEM((n, blocks, npad), F32),
            pltpu.VMEM((n * slot_keys, 128), BF16),
            pltpu.VMEM((rows, 128), BF16),
            pltpu.VMEM((128, rows), BF16),
            pltpu.VMEM((n, slot_keys, 128), BF16),
            pltpu.VMEM((n, 128, slot_keys), BF16),
            pltpu.VMEM((n, slot_keys, 128), BF16),
            pltpu.VMEM((n, 128, slot_keys), BF16),
            pltpu.VMEM((blocks, 2, lanes_all, 128), BF16),
            pltpu.VMEM((blocks, 2, 1, lanes_all), F32),
            pltpu.VMEM((blocks, 2, 1, lanes_all), F32),
            pltpu.VMEM((blocks, 2, HEAD_DIM, lanes_all), F32),
            pltpu.VMEM((rows, heads * HEAD_DIM), BF16),
            pltpu.VMEM((pieces, mine // pieces, width), F32),
            pltpu.VMEM((pieces, mine // pieces, width), F32),
            dma((4 + heads,)),
            dma((2,)),
            dma((n,)),
            dma((n,)),
            dma((n,)),
            dma((n,)),
            dma((n,)),
            dma((n,)),
            dma((pieces,)),
            dma((pieces,)),
        ],
        compiler_params=pltpu.CompilerParams(
            collective_id=0, has_side_effects=True, vmem_limit_bytes=48 * 1024 * 1024
        ),
    )(chosen, tokens, w_query, w_key, w_value, w_out)


def solution(mesh):
    placed = (
        P("dp", ("kv", "tp"), None),
        P(None, "tp"),
        P(None, "tp"),
        P(None, "tp"),
        P("tp", None),
        P("dp", "kv", None),
    )
    return jax.shard_map(
        shards,
        mesh=mesh,
        in_specs=placed,
        out_specs=(P("dp", ("kv", "tp"), None), P("dp", "kv", "tp")),
        check_vma=False,
    )
```

time: 162 us -> 45.1 us (0.28); the launches traced: 159 us -> 44.7 us
  local copies, waits for them, and re-layouts: 68.4 us -> 7.57 us
  Pallas kernels: 0 us -> 36.5 us
  matrix products: 24.8 us -> 0 us
  waiting for transfers between devices: 19 us -> 0 us
  starting transfers between devices: 16.3 us -> 0 us
  other arithmetic: 15.5 us -> 0 us
  between operations: 14.3 us -> 0.65 us
    pallas_call x0 -> x1, Pallas kernels: none -> 36.5 us  [shards(): pl.pallas_call(functools.partial(kernel, n), out_shape=(jax.ShapeDtypeStr...]
    gather x20 -> x0, local copies, waits for them, and re-layouts: 29.9 us -> none  [the longest x8 12.3 us: one_block(): got_values[block_slots].reshape(PICK * BLK, kv_count, HEAD_DIM)]
    dot_general x20 -> x0, matrix products: 24.8 us -> none  [the longest x8 11.5 us: one_block(): jnp.einsum('qkgd,nkd->kgqn', block_queries, gathered_keys, preferred_elem...]
    all_to_all x3 -> x0, starting transfers between devices: 16.2 us -> none  [the longest x1 7.17 us: shards(): lax.all_to_all(send_values, 'kv', split_axis=0, concat_axis=0, tiled=True)]
    reduce_scatter x1 -> x0, waiting for transfers between devices: 11.6 us -> none  [own_rows(): return lax.psum_scatter(whole, axis, scatter_dimension=0, tiled=True)]
    reshape x17 -> x0, local copies, waits for them, and re-layouts: 11.5 us -> none  [the longest x8 5.71 us: one_block(): got_values[block_slots].reshape(PICK * BLK, kv_count, HEAD_DIM)]
    dynamic_slice x32 -> x0, local copies, waits for them, and re-layouts: 7.96 us -> none  [shards(): lax.map(one_block, (query_blocks, key_blocks, value_blocks, slot_index, u...]
    dynamic_update_slice x24 -> x0, local copies, waits for them, and re-layouts: 6.21 us -> none  [shards(): lax.map(one_block, (query_blocks, key_blocks, value_blocks, slot_index, u...]
  transfers between devices with their start and end apart: 5 -> 0, of which waited for: 4 -> 0; matrix products, arithmetic and copies ran while one was open for 9% -> 0% of each run, Pallas kernels for 0% -> 0%
where the time goes in v1:
time: 45.1 us; the launch traced here: 44.7 us
  Pallas kernels  36.5 us (81%)
  local copies, waits for them, and re-layouts  7.57 us (17%)
  between operations  0.65 us (1%)
    pallas_call x1, Pallas kernels, shards(): pl.pallas_call(functools.partial(kernel, n), out_shape=(jax.ShapeDtypeStr...  36.5 us
    unnamed x13, local copies, waits for them, and re-layouts  6.86 us

profile of v1, /device:TPU:27, one launch (start us, length us, event | category | flops | bytes accessed | tf_op | source)
XLA Modules:
  0.0 44.7 jit_solution(7500507528494063975)
XLA Ops:
  0.6 0.0 copy-start
  0.6 1.2 %copy-done = bf16[1024,512]{1,0:T(8,128)(2,1)S(1)} copy-done((bf16[1024,512]{1,0:T(8,128)(2,1)S(1)}, bf16[1024,512]{1,0:T(8,128)(2,1)}, u32[]{:S(2)}) %copy-start) | copy-done | bytes 1048600
  1.9 0.0 copy-start.1
  1.9 1.2 %copy-done.1 = bf16[512,1024]{1,0:T(8,128)(2,1)S(1)} copy-done((bf16[512,1024]{1,0:T(8,128)(2,1)S(1)}, bf16[512,1024]{1,0:T(8,128)(2,1)}, u32[]{:S(2)}) %copy-start.1) | copy-done | bytes 1048600
  3.1 0.0 copy-start.2
  3.1 1.0 %copy-done.2 = bf16[1,256,1024]{2,1,0:T(8,128)(2,1)S(1)} copy-done((bf16[1,256,1024]{2,1,0:T(8,128)(2,1)S(1)}, bf16[1,256,1024]{2,1,0:T(8,128)(2,1)}, u32[]{:S(2)}) %copy-start.2) | copy-done | bytes 524312
  4.1 0.0 copy-start.3
  4.1 0.9 %copy-done.3 = bf16[1024,128]{1,0:T(8,128)(2,1)S(1)} copy-done((bf16[1024,128]{1,0:T(8,128)(2,1)S(1)}, bf16[1024,128]{1,0:T(8,128)(2,1)}, u32[]{:S(2)}) %copy-start.3) | copy-done | bytes 262168
  5.1 0.0 copy-start.4
  5.1 0.9 %copy-done.4 = bf16[1024,128]{1,0:T(8,128)(2,1)S(1)} copy-done((bf16[1024,128]{1,0:T(8,128)(2,1)S(1)}, bf16[1024,128]{1,0:T(8,128)(2,1)}, u32[]{:S(2)}) %copy-start.4) | copy-done | bytes 262168
  6.0 0.0 copy-start.5
  6.0 0.7 %copy-done.5 = s32[1,8,15]{2,1,0:T(8,128)S(1)} copy-done((s32[1,8,15]{2,1,0:T(8,128)S(1)}, s32[1,8,15]{2,1,0:T(8,128)}, u32[]{:S(2)}) %copy-start.5) | copy-done | bytes 504
  6.7 36.5 %shard_map.77 = (bf16[1,256,1024]{2,1,0:T(8,128)(2,1)S(1)}, f32[1,512,8]{2,1,0:T(8,128)S(1)}) custom-call(s32[1,8,15]{2,1,0:T(8,128)S(1)} %copy-done.5, bf16[1,256,1024]{2,1,0:T(8,128)(2,1)S(1)} %copy-done.2, bf16[1024,512]{1,0:T(8,128)(2,1)S(1)} %copy-done, bf16[1024,128]{1,0:T(8,128)(2,1)S(1)} %copy-done.3, bf16[1024,128]{1,0:T(8,128)(2,1)S(1)} %copy-done.4, ...), custom_call_target="tpu_custom_call" | custom-call | tf_op jit(solution)/shard_map/pallas_call | solution.py:387
  43.2 0.7 %copy.8 = f32[1,512,8]{1,2,0:T(8,128)} copy(f32[1,512,8]{2,1,0:T(8,128)S(1)} %get-tuple-element.3) | data formatting | bytes 32768 | tf_op jit(solution)/shard_map/pallas_call | solution.py:387
  43.9 0.8 %copy.10 = bf16[1,256,1024]{2,1,0:T(8,128)(2,1)} copy(bf16[1,256,1024]{2,1,0:T(8,128)(2,1)S(1)} %get-tuple-element.6) | data formatting | bytes 1048576
Async XLA Ops:
  0.6 1.2 %copy-start = (bf16[1024,512]{1,0:T(8,128)(2,1)S(1)}, bf16[1024,512]{1,0:T(8,128)(2,1)}, u32[]{:S(2)}) copy-start(bf16[1024,512]{1,0:T(8,128)(2,1)} %wq_hbm.1) | copy-start | bytes 3145732
  1.9 1.2 %copy-start.1 = (bf16[512,1024]{1,0:T(8,128)(2,1)S(1)}, bf16[512,1024]{1,0:T(8,128)(2,1)}, u32[]{:S(2)}) copy-start(bf16[512,1024]{1,0:T(8,128)(2,1)} %wo_hbm.1) | copy-start | bytes 3145732
  3.1 1.0 %copy-start.2 = (bf16[1,256,1024]{2,1,0:T(8,128)(2,1)S(1)}, bf16[1,256,1024]{2,1,0:T(8,128)(2,1)}, u32[]{:S(2)}) copy-start(bf16[1,256,1024]{2,1,0:T(8,128)(2,1)} %tokens_hbm.1) | copy-start | bytes 1572868
  4.1 0.9 %copy-start.3 = (bf16[1024,128]{1,0:T(8,128)(2,1)S(1)}, bf16[1024,128]{1,0:T(8,128)(2,1)}, u32[]{:S(2)}) copy-start(bf16[1024,128]{1,0:T(8,128)(2,1)} %wk_hbm.1) | copy-start | bytes 786436
  5.1 0.9 %copy-start.4 = (bf16[1024,128]{1,0:T(8,128)(2,1)S(1)}, bf16[1024,128]{1,0:T(8,128)(2,1)}, u32[]{:S(2)}) copy-start(bf16[1024,128]{1,0:T(8,128)(2,1)} %wv_hbm.1) | copy-start | bytes 786436
  6.0 0.7 %copy-start.5 = (s32[1,8,15]{2,1,0:T(8,128)S(1)}, s32[1,8,15]{2,1,0:T(8,128)}, u32[]{:S(2)}) copy-start(s32[1,8,15]{2,1,0:T(8,128)} %chosen_ref.1) | copy-start | bytes 1444

commit v2 on v1

--- a/solution.py
+++ b/solution.py
@@ -53,6 +53,9 @@
     sel_v,
     got_k,
     got_v,
+    hot_s,
+    q_raw,
+    v_blk,
     qaug,
     m_s,
     l_s,
@@ -187,32 +190,45 @@
         )
         return x * cos_t[part] + turned * sin_t[part]
 
-    ld_k.wait()
-    ld_v.wait()
-
-    def project_kv(part):
-        out = mm(tok[part], wkv[...]).astype(BF16)
-        keys[part] = rope(out[:, 0:128].astype(F32), part).astype(BF16)
-        return out[:, 128:256]
-
-    mine_part = pl.ds(pl.multiple_of(half * mine, mine), mine)
-    other_part = pl.ds(pl.multiple_of(other * mine, mine), mine)
-    v_mine = project_kv(mine_part).astype(F32).T.astype(BF16)
-    vals_t[:, mine_part] = v_mine
-    tok_copy.wait_recv()
-    v_other = project_kv(other_part).astype(F32).T.astype(BF16)
-    vals_t[:, other_part] = v_other
-
-    def select(tab, d):
+    def selector(tab, d):
         first = (
             iota((slot_keys, nslots), 1) == me * CAP + iota((slot_keys, nslots), 0) // BLK
         ).astype(BF16)
         last = (iota((npad, rows), 0) == me * blocks + iota((npad, rows), 1) // BLK).astype(BF16)
         chain = mm(mm(first, tab).astype(BF16), last)
         same = iota((slot_keys, rows), 0) % BLK == iota((slot_keys, rows), 1) % BLK
-        hot = jnp.where(same, chain, 0.0).astype(BF16)
-        sel_k[d] = mm(hot, keys[...]).astype(BF16)
-        sel_v[d] = mm(vals_t[...], hot, NT).astype(BF16)
+        hot_s[d] = jnp.where(same, chain, 0.0).astype(BF16)
+
+    selector(table, 0)
+
+    own_part = pl.ds(pl.multiple_of(half * mine, mine), mine)
+    far_part = pl.ds(pl.multiple_of(other * mine, mine), mine)
+
+    def project_kv(part):
+        out = mm(tok[part], wkv[...]).astype(BF16)
+        keys[part] = rope(out[:, 0:128].astype(F32), part).astype(BF16)
+        vals_t[:, part] = out[:, 128:256].astype(F32).T.astype(BF16)
+
+    def project_q(part):
+        q_raw[part] = mm(tok[part], wq[...]).astype(BF16)
+
+    ld_k.wait()
+    ld_v.wait()
+    project_kv(own_part)
+    ld_q.wait()
+    project_q(own_part)
+
+    @pl.loop(1, n - me)
+    def _(d):
+        pick_copy(d, me).wait_recv()
+        selector(slot_table(pick[d]), d)
+
+    tok_copy.wait_recv()
+    project_kv(far_part)
+
+    def select(d):
+        sel_k[d] = mm(hot_s[d], keys[...]).astype(BF16)
+        sel_v[d] = mm(vals_t[...], hot_s[d], NT).astype(BF16)
 
     def key_copy(d, target):
         return pltpu.make_async_remote_copy(
@@ -236,19 +252,18 @@
 
     @pl.loop(1, n - me)
     def _(d):
-        pick_copy(d, me).wait_recv()
-        select(slot_table(pick[d]), d)
+        select(d)
         key_copy(d, me + d).start()
         value_copy(d, me + d).start()
 
-    select(table, 0)
-
-    ld_q.wait()
-
-    @pl.loop(0, blocks)
-    def _(c):
-        part = pl.ds(pl.multiple_of(c * BLK, BLK), BLK)
-        q = mm(tok[part], wq[...]).astype(BF16).astype(F32)
+    project_q(far_part)
+    select(0)
+    for c in range(blocks):
+        v_blk[c] = vals_t[:, c * BLK : (c + 1) * BLK]
+
+    for c in range(blocks):
+        part = slice(c * BLK, (c + 1) * BLK)
+        q = q_raw[part].astype(F32)
         tiles = [
             rope(q[:, t * 128 : (t + 1) * 128], part) * HEAD_DIM**-0.5 for t in range(groups)
         ]
@@ -268,31 +283,40 @@
         low = iota(k.shape, 1) < 64
         return jnp.where(low, k, extra) if h == 0 else jnp.where(low, extra, k)
 
+    group = 2 if blocks % 2 == 0 else 1
+
+    def tiles_of(i):
+        return [(i * group + u, h) for u in range(group) for h in range(2)]
+
+    def head_of(h):
+        return slice(h * HEAD_DIM, (h + 1) * HEAD_DIM)
+
     own_bias = bias[pl.ds(pl.multiple_of(me * slot_keys, slot_keys), slot_keys)]
-
-    @pl.loop(0, blocks)
-    def _(c):
-        part = pl.ds(pl.multiple_of(c * BLK, BLK), BLK)
-        for h in range(2):
+    k_slots = [widened(sel_k[0], own_bias, h) for h in range(2)]
+    ok = iota((BLK, lanes_all), 0) <= iota((BLK, lanes_all), 1) % BLK
+
+    @pl.loop(0, blocks // group)
+    def _(i):
+        done = []
+        for c, h in tiles_of(i):
             q = qaug[c, h]
-            s = mm(widened(sel_k[0], own_bias, h), q, NT)
-            k_own = keys[part]
+            k_own = keys[pl.ds(pl.multiple_of(c * BLK, BLK), BLK)]
+            s = mm(k_slots[h], q, NT)
             s_own = mm(widened(k_own, jnp.zeros_like(k_own), h), q, NT)
-            ok = iota((BLK, lanes_all), 0) <= iota((BLK, lanes_all), 1) % BLK
             s_own = jnp.where(ok, s_own, NEGATIVE)
             m = jnp.maximum(
                 jnp.max(s, axis=0, keepdims=True), jnp.max(s_own, axis=0, keepdims=True)
             )
             p = jnp.exp(s - m)
             p_own = jnp.exp(s_own - m)
+            l = jnp.sum(p, axis=0, keepdims=True) + jnp.sum(p_own, axis=0, keepdims=True)
+            o = mm(sel_v[0, head_of(h)], p.astype(BF16))
+            o = o + mm(v_blk[c, head_of(h)], p_own.astype(BF16))
+            done.append((m, l, o))
+        for (c, h), (m, l, o) in zip(tiles_of(i), done):
             m_s[c, h] = m
-            l_s[c, h] = jnp.sum(p, axis=0, keepdims=True) + jnp.sum(p_own, axis=0, keepdims=True)
-            head = slice(h * HEAD_DIM, (h + 1) * HEAD_DIM)
-            block_hot = (
-                iota((BLK, rows), 1) == c * BLK + iota((BLK, rows), 0)
-            ).astype(BF16)
-            v_own = mm(vals_t[head], block_hot, NT).astype(BF16)
-            acc[c, h] = mm(sel_v[0, head], p.astype(BF16)) + mm(v_own, p_own.astype(BF16))
+            l_s[c, h] = l
+            acc[c, h] = o
 
     @pl.loop(1, me + 1)
     def _(d):
@@ -302,22 +326,25 @@
         extra = bias[pl.ds(pl.multiple_of(owner * slot_keys, slot_keys), slot_keys)]
         ks = [widened(got_k[d], extra, h) for h in range(2)]
 
-        @pl.loop(0, blocks)
-        def _(c):
-            for h in range(2):
+        @pl.loop(0, blocks // group)
+        def _(i):
+            done = []
+            held = [(m_s[c, h], l_s[c, h], acc[c, h]) for c, h in tiles_of(i)]
+            for (c, h), (m_old, l_old, o_old) in zip(tiles_of(i), held):
                 s = mm(ks[h], qaug[c, h], NT)
-                m_old = m_s[c, h]
                 m = jnp.maximum(m_old, jnp.max(s, axis=0, keepdims=True))
                 shrink = jnp.exp(m_old - m)
                 p = jnp.exp(s - m)
+                l = l_old * shrink + jnp.sum(p, axis=0, keepdims=True)
+                o = o_old * shrink + mm(got_v[d, head_of(h)], p.astype(BF16))
+                done.append((m, l, o))
+            for (c, h), (m, l, o) in zip(tiles_of(i), done):
                 m_s[c, h] = m
-                l_s[c, h] = l_s[c, h] * shrink + jnp.sum(p, axis=0, keepdims=True)
-                head = slice(h * HEAD_DIM, (h + 1) * HEAD_DIM)
-                acc[c, h] = acc[c, h] * shrink + mm(got_v[d, head], p.astype(BF16))
-
-    @pl.loop(0, blocks)
-    def _(c):
-        part = pl.ds(pl.multiple_of(c * BLK, BLK), BLK)
+                l_s[c, h] = l
+                acc[c, h] = o
+
+    for c in range(blocks):
+        part = slice(c * BLK, (c + 1) * BLK)
         sums = [l_s[c, h] for h in range(2)]
         both = jnp.concatenate([acc[c, h] / sums[h] for h in range(2)], axis=0).T
         for g in range(groups):
@@ -327,7 +354,7 @@
             [logs[h][:, g * BLK : (g + 1) * BLK] for h in range(2) for g in range(groups)],
             axis=0,
         )
-        logs_ref[0, part] = stacked.T
+        logs_ref[0, :, part] = stacked
 
     for copy in ld_o:
         copy.wait()
@@ -384,11 +411,11 @@
     dma = pltpu.SemaphoreType.DMA
     vmem = pl.BlockSpec(memory_space=pltpu.VMEM)
     hbm = pl.BlockSpec(memory_space=pl.ANY)
-    return pl.pallas_call(
+    normed, logs = pl.pallas_call(
         functools.partial(kernel, n),
         out_shape=(
             jax.ShapeDtypeStruct((1, mine, width), BF16),
-            jax.ShapeDtypeStruct((1, rows, heads), F32),
+            jax.ShapeDtypeStruct((1, heads, rows), F32),
         ),
         in_specs=[vmem, hbm, hbm, hbm, hbm, hbm],
         out_specs=(vmem, vmem),
@@ -407,6 +434,9 @@
             pltpu.VMEM((n, 128, slot_keys), BF16),
             pltpu.VMEM((n, slot_keys, 128), BF16),
             pltpu.VMEM((n, 128, slot_keys), BF16),
+            pltpu.VMEM((n, slot_keys, rows), BF16),
+            pltpu.VMEM((rows, w_query.shape[1]), BF16),
+            pltpu.VMEM((blocks, 128, BLK), BF16),
             pltpu.VMEM((blocks, 2, lanes_all, 128), BF16),
             pltpu.VMEM((blocks, 2, 1, lanes_all), F32),
             pltpu.VMEM((blocks, 2, 1, lanes_all), F32),
@@ -426,9 +456,10 @@
             dma((pieces,)),
         ],
         compiler_params=pltpu.CompilerParams(
-            collective_id=0, has_side_effects=True, vmem_limit_bytes=48 * 1024 * 1024
+            collective_id=0, has_side_effects=True, vmem_limit_bytes=67043328
         ),
     )(chosen, tokens, w_query, w_key, w_value, w_out)
+    return normed, jnp.swapaxes(logs, 1, 2)
 
 
 def solution(mesh):

time: 45.1 us -> 37.5 us (0.83)
  local copies, waits for them, and re-layouts: 7.57 us -> 2.48 us
  Pallas kernels: 36.5 us -> 33.9 us
    unnamed x13 -> x4, local copies, waits for them, and re-layouts: 6.86 us -> 2.48 us
    pallas_call x1, Pallas kernels: 36.5 us -> 33.9 us  [shards(): pl.pallas_call(functools.partial(kernel, n), out_shape=(jax.ShapeDtypeStr...]
    pallas_call x1 -> x0, local copies, waits for them, and re-layouts: 0.71 us -> none  [shards(): pl.pallas_call(functools.partial(kernel, n), out_shape=(jax.ShapeDtypeStr...]
where the time goes in v2:
time: 37.5 us; the launch traced here: 37 us
  Pallas kernels  33.9 us (90%)
  local copies, waits for them, and re-layouts  2.48 us (7%)
  between operations  0.65 us (2%)
    pallas_call x1, Pallas kernels, shards(): pl.pallas_call(functools.partial(kernel, n), out_shape=(jax.ShapeDtypeStr...  33.9 us
    unnamed x4, local copies, waits for them, and re-layouts  2.48 us

profile of v2, /device:TPU:27, one launch (start us, length us, event | category | flops | bytes accessed | tf_op | source)
XLA Modules:
  0.0 37.0 jit_solution(14084126973211530696)
XLA Ops:
  0.6 33.9 %shard_map.77 = (bf16[1,256,1024]{2,1,0:T(8,128)(2,1)}, f32[1,8,512]{2,1,0:T(8,128)}) custom-call(s32[1,8,15]{2,1,0:T(8,128)} %chosen_ref.1, bf16[1,256,1024]{2,1,0:T(8,128)(2,1)} %tokens_hbm.1, bf16[1024,512]{1,0:T(8,128)(2,1)} %wq_hbm.1, bf16[1024,128]{1,0:T(8,128)(2,1)} %wk_hbm.1, bf16[1024,128]{1,0:T(8,128)(2,1)} %wv_hbm.1, bf16[512,1024]{1,0:T(8,128)(2,1)} %wo_hbm.1), custom_call_target="tpu_custom_call" | custom-call | tf_op jit(solution)/shard_map/pallas_call | solution.py:414
  34.5 0.0 copy-start
  34.5 1.9 %copy.10 = bf16[1,256,1024]{2,1,0:T(8,128)(2,1)} copy(bf16[1,256,1024]{2,1,0:T(8,128)(2,1)} %get-tuple-element.8) | data formatting | bytes 1048576
  36.4 0.0 copy-done
  36.4 0.6 %copy.11 = f32[1,512,8]{1,2,0:T(8,128)} copy(f32[1,512,8]{1,2,0:T(8,128)S(1)} %bitcast.1) | data formatting | bytes 32768
Async XLA Ops:
  34.5 1.9 %copy-start = (f32[1,8,512]{2,1,0:T(8,128)S(1)}, f32[1,8,512]{2,1,0:T(8,128)}, u32[]{:S(2)}) copy-start(f32[1,8,512]{2,1,0:T(8,128)} %get-tuple-element.5) | copy-start | bytes 49156

commit v3 on v2

--- a/solution.py
+++ b/solution.py
@@ -209,14 +209,9 @@
         keys[part] = rope(out[:, 0:128].astype(F32), part).astype(BF16)
         vals_t[:, part] = out[:, 128:256].astype(F32).T.astype(BF16)
 
-    def project_q(part):
-        q_raw[part] = mm(tok[part], wq[...]).astype(BF16)
-
     ld_k.wait()
     ld_v.wait()
     project_kv(own_part)
-    ld_q.wait()
-    project_q(own_part)
 
     @pl.loop(1, n - me)
     def _(d):
@@ -251,12 +246,14 @@
         )
 
     @pl.loop(1, n - me)
-    def _(d):
+    def _(e):
+        d = n - me - e
         select(d)
         key_copy(d, me + d).start()
         value_copy(d, me + d).start()
 
-    project_q(far_part)
+    ld_q.wait()
+    q_raw[...] = mm(tok[...], wq[...]).astype(BF16)
     select(0)
     for c in range(blocks):
         v_blk[c] = vals_t[:, c * BLK : (c + 1) * BLK]

time: 37.5 us -> 37.1 us (0.989)
  Pallas kernels: 33.9 us -> 33.4 us
    pallas_call x1, Pallas kernels: 33.9 us -> 33.4 us  [shards(): pl.pallas_call(functools.partial(kernel, n), out_shape=(jax.ShapeDtypeStr...]
where the time goes in v3:
time: 37.1 us; the launch traced here: 36.6 us
  Pallas kernels  33.4 us (90%)
  local copies, waits for them, and re-layouts  2.48 us (7%)
  between operations  0.65 us (2%)
    pallas_call x1, Pallas kernels, shards(): pl.pallas_call(functools.partial(kernel, n), out_shape=(jax.ShapeDtypeStr...  33.4 us
    unnamed x4, local copies, waits for them, and re-layouts  2.48 us

profile of v3, /device:TPU:27, one launch (start us, length us, event | category | flops | bytes accessed | tf_op | source)
XLA Modules:
  0.0 36.6 jit_solution(3542166443291103020)
XLA Ops:
  0.6 33.4 %shard_map.77 = (bf16[1,256,1024]{2,1,0:T(8,128)(2,1)}, f32[1,8,512]{2,1,0:T(8,128)}) custom-call(s32[1,8,15]{2,1,0:T(8,128)} %chosen_ref.1, bf16[1,256,1024]{2,1,0:T(8,128)(2,1)} %tokens_hbm.1, bf16[1024,512]{1,0:T(8,128)(2,1)} %wq_hbm.1, bf16[1024,128]{1,0:T(8,128)(2,1)} %wk_hbm.1, bf16[1024,128]{1,0:T(8,128)(2,1)} %wv_hbm.1, bf16[512,1024]{1,0:T(8,128)(2,1)} %wo_hbm.1), custom_call_target="tpu_custom_call" | custom-call | tf_op jit(solution)/shard_map/pallas_call | solution.py:411
  34.1 0.0 copy-start
  34.1 1.9 %copy.10 = bf16[1,256,1024]{2,1,0:T(8,128)(2,1)} copy(bf16[1,256,1024]{2,1,0:T(8,128)(2,1)} %get-tuple-element.8) | data formatting | bytes 1048576
  35.9 0.0 copy-done
  36.0 0.6 %copy.11 = f32[1,512,8]{1,2,0:T(8,128)} copy(f32[1,512,8]{1,2,0:T(8,128)S(1)} %bitcast.1) | data formatting | bytes 32768
Async XLA Ops:
  34.1 1.9 %copy-start = (f32[1,8,512]{2,1,0:T(8,128)S(1)}, f32[1,8,512]{2,1,0:T(8,128)}, u32[]{:S(2)}) copy-start(f32[1,8,512]{2,1,0:T(8,128)} %get-tuple-element.5) | copy-start | bytes 49156
